TPU v7x, 32 devices: a whole 2x2x4 slice. The times are simulated.
32 devices in a mesh: ep: 4 (over y, x), tp: 8 (over z, core).
Axes of the slice: x: 2, y: 2, z: 4, core: 2. Of those that a mesh axis runs over, the one named last changes fastest.
Arguments:
- pool_input: bfloat16 [4096, 1024], P('ep', 'tp'), may hold values from -6 to 6
- pool_gain: float32 [1024], P('tp'), may hold values from 0.1 to 1.9
- mix_weight: bfloat16 [1024, 2048], P('tp'), may hold values from -0.1875 to 0.1875
- moe_input: bfloat16 [8192, 2048], P(('ep', 'tp')), may hold values from -6 to 6
- moe_gain: float32 [2048], replicated, may hold values from 0.1 to 1.9
- expert_ids: int32 [8192, 2], P(('ep', 'tp')), may hold values from 0 to 15, as said below
- route_weight: float32 [8192, 2], P(('ep', 'tp')), may hold values from 0.2 to 1
- gate_weight: bfloat16 [16, 2048, 1024], P('ep', None, 'tp'), may hold values from -0.125 to 0.125
- up_weight: bfloat16 [16, 2048, 1024], P('ep', None, 'tp'), may hold values from -0.125 to 0.125
- down_weight: bfloat16 [16, 2048, 1024], P('ep', None, 'tp'), may hold values from -0.1875 to 0.1875
Outputs:
- mixed_out: bfloat16 [4096, 2048], P(('ep', 'tp'))
- moe_out: bfloat16 [8192, 2048], P(('ep', 'tp'))
Inputs may be any that keep to these rules, and one draw needn't show every extreme that they name: `expert_ids`: each row names 2 different experts of one group of 4 consecutive experts. In each aligned block of 256 rows (the rows of one device) no expert is named by more than 48 rows, and some expert is named by exactly 48 rows.
All inputs are finite; a program needn't handle non-finite values.
Results may differ from a plain program's by a relative error of at most 0.012.
Values may be sent and summed in bfloat16 or wider, within the bound.
A program may use at most 128 MiB of HBM per device.

v0:
```python
import jax
import jax.numpy as jnp
from jax import lax
from jax.sharding import PartitionSpec as P

GROUP_CH = 256
EXPERTS = 16
GROUP_EXP = 4
TOP = 2
CAP = 48
eps_norm = 1e-06


def from_behind(shard, axis, by):
    peers = lax.axis_size(axis)
    pairs = [(i, i + by) for i in range(peers) if 0 <= i + by < peers]
    return lax.ppermute(shard, axis, pairs)


def window_sums(extended, row_count):
    level_sum = extended
    stride = 1
    outputs = []
    for doubling in range(4):
        level_sum = level_sum[stride:] + level_sum[:-stride]
        stride = stride * 2
        outputs.append(level_sum[level_sum.shape[0] - row_count :])
    return outputs


def pool_mixer(pool_input, pool_gain):
    row_count, channels = pool_input.shape
    carried = from_behind(pool_input[row_count - 15 :], "ep", 1)
    extended = jnp.concatenate([carried, pool_input], axis=0).astype(jnp.float32)
    window_list = window_sums(extended, row_count)
    channel_ids = lax.axis_index("tp") * channels + lax.iota(jnp.int32, channels)
    group_ids = channel_ids // GROUP_CH
    position = lax.axis_index("ep") * row_count + lax.iota(jnp.int32, row_count)
    summed = jnp.zeros((row_count, channels), jnp.float32)
    widths = jnp.zeros((channels,), jnp.int32)
    for index_group in range(4):
        inside = group_ids == index_group
        summed = jnp.where(inside[None, :], window_list[index_group], summed)
        widths = jnp.where(inside, 2 ** (index_group + 1), widths)
    counted = jnp.minimum(position[:, None] + 1, widths[None, :]).astype(jnp.float32)
    values = extended[15:]
    return ((summed / counted - values) * pool_gain).astype(jnp.bfloat16)


def dispatch_plan(expert_ids, route_weight, ep_size):
    local_experts = EXPERTS // ep_size
    share = TOP if local_experts % GROUP_EXP == 0 else 1
    capacity = local_experts * CAP // share
    owners = expert_ids // local_experts
    ep_index = lax.iota(jnp.int32, ep_size)
    member = jnp.any(owners[:, :, None] == ep_index[None, None, :], axis=1)
    counts = member.astype(jnp.int32)
    rank = jnp.cumsum(counts, axis=0) - counts
    slot = jnp.where(member, rank, -1).T
    placing = slot[:, None, :] == lax.iota(jnp.int32, capacity)[None, :, None]
    dense_weight = jnp.sum(
        jnp.where(
            expert_ids[:, :, None] == lax.iota(jnp.int32, EXPERTS)[None, None, :],
            route_weight[:, :, None],
            0.0,
        ),
        axis=1,
    )
    dense_weight = dense_weight.reshape(-1, ep_size, local_experts)
    slot_weight = jnp.einsum(
        "ecn,nej->ecj", placing.astype(jnp.float32), dense_weight, precision=lax.Precision.HIGHEST
    )
    return (placing.astype(jnp.bfloat16).reshape(ep_size * capacity, -1), slot_weight, capacity)


def body(
    pool_input,
    pool_gain,
    mix_weight,
    moe_input,
    moe_gain,
    expert_ids,
    route_weight,
    gate_weight,
    up_weight,
    down_weight,
):
    pooled = pool_mixer(pool_input, pool_gain)
    regrouped = lax.all_to_all(pooled, "tp", split_axis=0, concat_axis=1, tiled=True)
    mixed_sum = jnp.dot(
        regrouped,
        lax.all_gather(mix_weight, "tp", axis=0, tiled=True),
        preferred_element_type=jnp.float32,
    )
    mixed_out = mixed_sum.astype(jnp.bfloat16)
    inputs = moe_input.astype(jnp.float32)
    scale_rows = lax.rsqrt(jnp.mean(inputs * inputs, axis=-1, keepdims=True) + eps_norm)
    normed = (inputs * scale_rows * moe_gain).astype(jnp.bfloat16)
    ep_size = lax.axis_size("ep")
    placing, slot_weight, capacity = dispatch_plan(expert_ids, route_weight, ep_size)
    outgoing = jnp.dot(placing, normed, preferred_element_type=jnp.float32).astype(jnp.bfloat16)
    arrived = lax.all_to_all(outgoing, "ep", split_axis=0, concat_axis=0, tiled=True)
    weights = lax.all_to_all(slot_weight, "ep", split_axis=0, concat_axis=0, tiled=True)
    weights = weights.reshape(ep_size * capacity, -1)
    tokens = lax.all_gather(arrived, "tp", axis=0, tiled=True)
    weights = lax.all_gather(weights, "tp", axis=0, tiled=True)
    gate_part = jnp.einsum("nd,edf->enf", tokens, gate_weight, preferred_element_type=jnp.float32)
    upward = jnp.einsum("nd,edf->enf", tokens, up_weight, preferred_element_type=jnp.float32)
    hidden = (jax.nn.silu(gate_part) * upward * weights.T[:, :, None]).astype(jnp.bfloat16)
    partial = jnp.einsum("enf,edf->nd", hidden, down_weight, preferred_element_type=jnp.float32)
    reduced = lax.psum_scatter(partial.astype(jnp.bfloat16), "tp", scatter_dimension=0, tiled=True)
    returned = lax.all_to_all(reduced, "ep", split_axis=0, concat_axis=0, tiled=True)
    combined = lax.dot_general(
        placing, returned, (((0,), (0,)), ((), ())), preferred_element_type=jnp.float32
    )
    moe_out = combined.astype(jnp.bfloat16)
    return (mixed_out, moe_out)


def solution(mesh):
    return jax.shard_map(
        body,
        mesh=mesh,
        in_specs=(
            P("ep", "tp"),
            P("tp"),
            P("tp", None),
            P(("ep", "tp"), None),
            P(),
            P(("ep", "tp"), None),
            P(("ep", "tp"), None),
            P("ep", None, "tp"),
            P("ep", None, "tp"),
            P("ep", None, "tp"),
        ),
        out_specs=(P(("ep", "tp"), None), P(("ep", "tp"), None)),
        check_vma=False,
    )
```

profile of v0, /device:TPU:0, one launch (start us, length us, event | category | flops | bytes accessed | tf_op | source)
XLA Modules:
  0.0 379.1 jit_solution(9585453362862034271)
XLA Ops:
  7.2 0.0 copy-start
  7.2 0.0 all-gather.5.cloned.1.call-start
  7.2 0.8 and_select_fusion
  8.1 1.2 reduce-window.6
  9.3 0.1 slice.68
  9.4 0.1 copy.31
  9.5 0.1 copy.32
  9.6 0.1 add_bitcast_fusion
  9.7 0.1 eq.111
  9.8 1.5 fusion.16
  11.3 0.1 bitcast_compare_fusion
  11.5 0.0 copy-start.2
  11.5 0.0 copy-start.3
  11.5 1.9 convolution_convert_fusion
  13.4 24.9 %all_to_all.45 = bf16[4,96,2048]{2,1,0:T(8,128)(2,1)} all-to-all(bf16[4,96,2048]{2,1,0:T(8,128)(2,1)S(1)} %bitcast.72), channel_id=1, replica_groups=mesh['ep'=4,'tp'=8] {'ep'}, dimensions={0} | all-to-all | bytes 3145728 | tf_op jit(solution)/shard_map/all_to_all | solution.py:102
  38.3 0.0 all-gather.5.cloned.1.call-update
  38.3 0.0 reduce-scatter.2.cloned.1.call-start
  38.4 0.0 copy-done.2
  38.4 0.0 copy-done.3
  38.4 0.3 fusion.28
  38.7 7.0 %all_to_all.46 = f32[4,96,4]{1,2,0:T(4,128)S(1)} all-to-all(f32[4,96,4]{1,2,0:T(4,128)S(1)} %fusion.28), channel_id=1, replica_groups=mesh['ep'=4,'tp'=8] {'ep'}, dimensions={0} | all-to-all | bytes 12288 | tf_op jit(solution)/shard_map/all_to_all | solution.py:103
  45.7 0.1 reshape.89
  45.8 17.4 %all_gather.11 = f32[3072,4]{0,1:T(4,128)S(1)} all-gather(f32[384,4]{0,1:T(4,128)S(1)} %reshape.89), channel_id=1, replica_groups=mesh['ep'=4,'tp'=8] {'tp'}, dimensions={0}, use_global_device_ids=true | all-gather | bytes 55296 | tf_op jit(solution)/shard_map/all_gather | solution.py:106
  63.2 92.0 %all-gather.5.cloned.1.call-done = bf16[3072,2048]{1,0:T(8,128)(2,1)} async-done(((bf16[384,2048]{1,0:T(8,128)(2,1)}), bf16[3072,2048]{1,0:T(8,128)(2,1)}) %all-gather.5.cloned.1.call-update) | async-done | bytes 12582928 | tf_op jit(solution)/shard_map/all_gather | solution.py:105
  155.2 12.0 %fusion.2 = f32[3072,4,128]{2,0,1:T(8,128)} fusion(bf16[4,2048,128]{2,1,0:T(8,128)(2,1)} %param.17, bf16[3072,2048]{1,0:T(8,128)(2,1)} %all-gather.5.cloned.1.call-done), kind=kOutput, calls=%fused_computation.3 | convolution fusion | flops 6442450944 | bytes 20971520 | tf_op jit(solution)/shard_map/nd,edf->enf/dot_general | solution.py:107
  167.2 0.0 copy-done
  167.2 19.4 %bitcast_convert_fusion = bf16[3072,2048]{1,0:T(8,128)(2,1)} fusion(bf16[4,2048,128]{2,1,0:T(8,128)(2,1)S(1)} %copy-done, f32[3072,4,128]{2,0,1:T(8,128)} %fusion.2, bf16[4,2048,128]{2,1,0:T(8,128)(2,1)} %param.18, bf16[3072,2048]{1,0:T(8,128)(2,1)} %all-gather.5.cloned.1.call-done, f32[4,3072]{1,0:T(4,128)S(1)} %bitcast.77), kind=kOutput, calls=%fused_computation | convolution fusion | flops 12902203392 | bytes 35700736 | tf_op jit(solution)/shard_map/enf,edf->nd/dot_general | solution.py:110
  186.6 0.0 copy-start.1
  186.6 0.0 reduce-scatter.2.cloned.1.call-update
  186.6 0.0 copy-start.4
  186.6 0.0 all-gather.3.cloned.1.call-start
  186.7 0.7 all-gather.3.cloned.1.call-update
  187.4 0.2 copy-done.1
  187.6 3.3 collective-permute-start
  190.9 1.2 collective-permute-done
  192.2 0.1 maximum_convert_fusion
  192.2 0.1 slice_add_fusion.1
  192.3 0.1 slice_add_fusion
  192.4 0.1 slice_add_fusion.2
  192.4 0.0 copy-done.4
  192.4 0.4 fusion.23
  192.8 16.7 %all_to_all.47 = bf16[8,128,128]{2,1,0:T(8,128)(2,1)S(1)} all-to-all(bf16[8,128,128]{2,1,0:T(8,128)(2,1)S(1)} %bitcast.74), channel_id=1, replica_groups=mesh['ep'=4,'tp'=8] {'tp'}, dimensions={0} | all-to-all | bytes 524288 | tf_op jit(solution)/shard_map/all_to_all | solution.py:89
  209.5 108.7 %reduce-scatter.2.cloned.1.call-done = bf16[384,2048]{1,0:T(8,128)(2,1)} async-done(((bf16[3072,2048]{1,0:T(8,128)(2,1)}), bf16[384,2048]{1,0:T(8,128)(2,1)}) %reduce-scatter.2.cloned.1.call-update) | async-done | bytes 1572880 | tf_op jit(solution)/shard_map/reduce_scatter | solution.py:111
  318.2 4.3 %all-to-all-start.3 = ((bf16[4,96,2048]{2,1,0:T(8,128)(2,1)}), bf16[4,96,2048]{2,1,0:T(8,128)(2,1)}, u32[]{:S(2)}, u32[]{:S(2)}) async-start(bf16[4,96,2048]{2,1,0:T(8,128)(2,1)} %bitcast.73), calls=%async_computation.4 | async-start | bytes 3145728 | tf_op jit(solution)/shard_map/all_to_all | solution.py:112
  322.6 0.2 copy.30
  322.7 42.9 %all-gather.3.cloned.1.call-done = bf16[1024,2048]{1,0:T(8,128)(2,1)} async-done(((bf16[128,2048]{1,0:T(8,128)(2,1)}), bf16[1024,2048]{1,0:T(8,128)(2,1)}) %all-gather.3.cloned.1.call-update) | async-done | bytes 4194320 | tf_op jit(solution)/shard_map/all_gather | solution.py:92
  365.7 3.7 convolution_convert_fusion.1
  369.4 0.0 all-to-all-done.3
  369.4 3.1 fusion.15
  (16 shorter events, 0.2 us)
Async XLA Ops:
  7.2 160.0 %copy-start = (bf16[4,2048,128]{2,1,0:T(8,128)(2,1)S(1)}, bf16[4,2048,128]{2,1,0:T(8,128)(2,1)}, u32[]{:S(2)}) copy-start(bf16[4,2048,128]{2,1,0:T(8,128)(2,1)} %param.19) | copy-start | bytes 6291460
  7.2 148.0 %all-gather.5.cloned.1.call-start = ((), (), s32[]{:S(2)}) async-start(), calls=%async_computation.6 | async-start | bytes 14155776 | tf_op jit(solution)/shard_map/all_gather | solution.py:105
  11.5 26.9 %copy-start.2 = (s32[256,2]{0,1:T(2,128)S(1)}, s32[256,2]{0,1:T(2,128)}, u32[]{:S(2)}) copy-start(s32[256,2]{0,1:T(2,128)} %param.15) | copy-start | bytes 6148
  11.5 26.9 %copy-start.3 = (f32[256,2]{0,1:T(2,128)S(1)}, f32[256,2]{0,1:T(2,128)}, u32[]{:S(2)}) copy-start(f32[256,2]{0,1:T(2,128)} %param.16) | copy-start | bytes 6148
  38.3 279.9 %reduce-scatter.2.cloned.1.call-start = ((), (), s32[]{:S(2)}) async-start(), calls=%async_computation.7 | async-start | bytes 14155776 | tf_op jit(solution)/shard_map/reduce_scatter | solution.py:111
  186.6 0.9 copy-start.1
  186.6 5.8 %copy-start.4 = (f32[128]{0:T(128)S(1)}, f32[128]{0:T(128)}, u32[]{:S(2)}) copy-start(f32[128]{0:T(128)} %param.11) | copy-start | bytes 1540
  186.6 179.0 %all-gather.3.cloned.1.call-start = ((), (), s32[]{:S(2)}) async-start(), calls=%async_computation.5 | async-start | bytes 4718592 | tf_op jit(solution)/shard_map/all_gather | solution.py:92
  187.6 4.6 %collective-permute-start = (bf16[15,128]{1,0:T(8,128)(2,1)S(1)}, bf16[15,128]{1,0:T(8,128)(2,1)S(1)}, u32[]{:S(2)}, u32[]{:S(2)}) collective-permute-start(bf16[15,128]{1,0:T(8,128)(2,1)S(1)} %slice.43), channel_id=1, source_target_pairs={{0,8},{8,16},{16,24},{1,9},{9,17},{17,25},{2,10},{10,18},{18,26},{... | collective-permute-start | bytes 11528 | tf_op jit(solution)/shard_map/ppermute | solution.py:17
  318.2 51.2 %all-to-all-start.3 = ((bf16[4,96,2048]{2,1,0:T(8,128)(2,1)}), bf16[4,96,2048]{2,1,0:T(8,128)(2,1)}, u32[]{:S(2)}, u32[]{:S(2)}) async-start(bf16[4,96,2048]{2,1,0:T(8,128)(2,1)} %bitcast.73), calls=%async_computation.4 | async-start | bytes 3145728 | tf_op jit(solution)/shard_map/all_to_all | solution.py:112
Sparse Core Ops, SparseCore 0:
  38.4 116.7 all-gather.4
  186.7 131.4 reduce-scatter.1
  319.8 45.8 all-gather.2
where the time goes:
time: 380 us; the launch traced here: 379 us
  waiting for transfers between devices  246 us (65%)
  blocking collectives  65.9 us (17%)
  matrix products  40.5 us (11%)
  between operations  13.9 us (4%)
  starting transfers between devices  7.76 us (2%)
  other arithmetic  4.48 us (1%)
    reduce_scatter x1, waiting for transfers between devices, body(): lax.psum_scatter(partial.astype(jnp.bfloat16), 'tp', scatter_dimension=0,...  109 us
    all_gather x1, waiting for transfers between devices, body(): tokens = lax.all_gather(arrived, 'tp', axis=0, tiled=True)  92 us
    all_gather x1, waiting for transfers between devices, body(): lax.all_gather(mix_weight, 'tp', axis=0, tiled=True)  42.9 us
    all_to_all x1, blocking collectives, body(): lax.all_to_all(outgoing, 'ep', split_axis=0, concat_axis=0, tiled=True)  24.9 us
    dot_general x1, matrix products, body(): jnp.einsum('enf,edf->nd', hidden, down_weight, preferred_element_type=jnp...  19.4 us
    all_gather x1, blocking collectives, body(): weights = lax.all_gather(weights, 'tp', axis=0, tiled=True)  17.4 us
    all_to_all x1, blocking collectives, body(): lax.all_to_all(pooled, 'tp', split_axis=0, concat_axis=1, tiled=True)  16.7 us
    dot_general x1, matrix products, body(): jnp.einsum('nd,edf->enf', tokens, gate_weight, preferred_element_type=jnp...  12 us
  transfers between devices with their start and end apart: 5, of which 4 were waited for; matrix products, arithmetic and copies ran while one was open for 1% of the time, Pallas kernels for 0%

commit v1 on v0

--- a/solution.py
+++ b/solution.py
@@ -102,8 +102,11 @@
     arrived = lax.all_to_all(outgoing, "ep", split_axis=0, concat_axis=0, tiled=True)
     weights = lax.all_to_all(slot_weight, "ep", split_axis=0, concat_axis=0, tiled=True)
     weights = weights.reshape(ep_size * capacity, -1)
-    tokens = lax.all_gather(arrived, "tp", axis=0, tiled=True)
-    weights = lax.all_gather(weights, "tp", axis=0, tiled=True)
+    tokens, weights = jnp.split(
+        lax.all_gather(jnp.concatenate([arrived, weights], axis=1), "tp", axis=0, tiled=True),
+        [arrived.shape[1]],
+        axis=1,
+    )
     gate_part = jnp.einsum("nd,edf->enf", tokens, gate_weight, preferred_element_type=jnp.float32)
     upward = jnp.einsum("nd,edf->enf", tokens, up_weight, preferred_element_type=jnp.float32)
     hidden = (jax.nn.silu(gate_part) * upward * weights.T[:, :, None]).astype(jnp.bfloat16)

time: 380 us -> 515 us (1.36)
  waiting for transfers between devices: 246 us -> 406 us
  blocking collectives: 65.9 us -> 16.7 us
  starting transfers between devices: 7.76 us -> 17.4 us
  matrix products: 40.5 us -> 46.2 us
    all_gather x1, waiting for transfers between devices: 92 us -> 233 us  [body(): lax.all_gather(jnp.concatenate([arrived, weights], axis=1), 'tp', axis=0,...]
    all_to_all x2 -> x0, blocking collectives: 31.9 us -> none  [the longest x1 24.9 us: body(): lax.all_to_all(outgoing, 'ep', split_axis=0, concat_axis=0, tiled=True)]
    all_to_all x0 -> x2, waiting for transfers between devices: none -> 19.1 us  [the longest x1 19.1 us: body(): lax.all_to_all(outgoing, 'ep', split_axis=0, concat_axis=0, tiled=True)]
    all_gather x1 -> x0, blocking collectives: 17.4 us -> none  [body(): weights = lax.all_gather(weights, 'tp', axis=0, tiled=True)]
    all_to_all x0 -> x2, starting transfers between devices: none -> 9.54 us  [the longest x1 5.19 us: body(): lax.all_to_all(slot_weight, 'ep', split_axis=0, concat_axis=0, tiled=True)]
  transfers between devices with their start and end apart: 5 -> 7, of which waited for: 4 -> 5; matrix products, arithmetic and copies ran while one was open for 1% -> 2% of each run, Pallas kernels for 0% -> 0%
where the time goes in v1:
time: 515 us; the launch traced here: 514 us
  waiting for transfers between devices  406 us (79%)
  matrix products  46.2 us (9%)
  starting transfers between devices  17.4 us (3%)
  blocking collectives  16.7 us (3%)
  between operations  13.9 us (3%)
  other arithmetic  9.02 us (2%)
  local copies, waits for them, and re-layouts  5.43 us (1%)
    all_gather x1, waiting for transfers between devices, body(): lax.all_gather(jnp.concatenate([arrived, weights], axis=1), 'tp', axis=0,...  233 us
    reduce_scatter x1, waiting for transfers between devices, body(): lax.psum_scatter(partial.astype(jnp.bfloat16), 'tp', scatter_dimension=0,...  109 us
    all_gather x1, waiting for transfers between devices, body(): lax.all_gather(mix_weight, 'tp', axis=0, tiled=True)  42.9 us
    dot_general x1, matrix products, body(): jnp.einsum('enf,edf->nd', hidden, down_weight, preferred_element_type=jnp...  21.3 us
    all_to_all x1, waiting for transfers between devices, body(): lax.all_to_all(outgoing, 'ep', split_axis=0, concat_axis=0, tiled=True)  19.1 us
    all_to_all x1, blocking collectives, body(): lax.all_to_all(pooled, 'tp', split_axis=0, concat_axis=1, tiled=True)  16.7 us
    dot_general x1, matrix products, body(): jnp.einsum('nd,edf->enf', tokens, gate_weight, preferred_element_type=jnp...  13.9 us
  transfers between devices with their start and end apart: 7, of which 5 were waited for; matrix products, arithmetic and copies ran while one was open for 2% of the time, Pallas kernels for 0%

profile of v1, /device:TPU:0, one launch (start us, length us, event | category | flops | bytes accessed | tf_op | source)
XLA Modules:
  0.0 514.5 jit_solution(16789781629966021948)
XLA Ops:
  7.2 0.0 copy-start
  7.2 0.8 and_select_fusion
  8.1 1.2 reduce-window.6
  9.3 0.1 slice.68
  9.4 0.1 copy.36
  9.5 0.1 copy.37
  9.6 0.1 add_bitcast_fusion
  9.7 0.7 select_reduce_fusion
  10.4 0.9 fusion.22
  11.3 5.2 %all-to-all-start.2 = ((f32[4,96,4]{1,2,0:T(4,128)}), f32[4,96,4]{1,2,0:T(4,128)S(1)}, u32[]{:S(2)}, u32[]{:S(2)}) async-start(f32[4,96,4]{1,2,0:T(4,128)} %fusion.22), calls=%async_computation.2 | async-start | bytes 16384 | tf_op jit(solution)/shard_map/all_to_all | solution.py:103
  16.5 0.1 eq.111
  16.6 0.1 bitcast_compare_fusion
  16.7 1.5 fusion.10
  18.2 3.1 convolution_convert_fusion
  21.3 0.0 all-to-all-done.2
  21.3 4.3 all-to-all-start.1
  25.7 0.0 all-gather.5.cloned.1.call-start
  25.7 0.1 copy.41
  25.9 19.1 %all-to-all-done.1 = bf16[4,96,2048]{2,1,0:T(8,128)(2,1)} async-done(((bf16[4,96,2048]{2,1,0:T(8,128)(2,1)}), bf16[4,96,2048]{2,1,0:T(8,128)(2,1)}, u32[]{:S(2)}, u32[]{:S(2)}) %all-to-all-start.1) | async-done | bytes 1572896 | tf_op jit(solution)/shard_map/all_to_all | solution.py:102
  45.0 1.8 bitcast_convert_fusion.1
  46.8 2.1 pad_maximum_fusion
  48.8 0.0 all-gather.5.cloned.1.call-update
  48.9 0.0 reduce-scatter.2.cloned.1.call-start
  48.9 233.1 %all-gather.5.cloned.1.call-done = f32[3072,2052]{1,0:T(8,128)} async-done(((f32[384,2052]{1,0:T(8,128)}), f32[3072,2052]{1,0:T(8,128)}) %all-gather.5.cloned.1.call-update) | async-done | bytes 25214992 | tf_op jit(solution)/shard_map/all_gather | solution.py:106
  282.0 2.6 slice_bitcast_fusion.7
  284.7 1.9 copy.40
  286.6 13.9 %fusion.1 = f32[3072,4,128]{2,0,1:T(8,128)} fusion(bf16[4,2048,128]{2,1,0:T(8,128)(2,1)} %param.17, f32[3072,2052]{1,0:T(8,128)} %all-gather.5.cloned.1.call-done), kind=kOutput, calls=%fused_computation.3 | convolution fusion | flops 6442450944 | bytes 20971520 | tf_op jit(solution)/shard_map/nd,edf->enf/dot_general | solution.py:110
  300.4 0.0 copy-done
  300.4 21.3 %bitcast_convert_fusion = bf16[3072,2048]{1,0:T(8,128)(2,1)} fusion(bf16[4,2048,128]{2,1,0:T(8,128)(2,1)S(1)} %copy-done, f32[3072,4,128]{2,0,1:T(8,128)} %fusion.1, bf16[4,2048,128]{2,1,0:T(8,128)(2,1)} %param.18, f32[3072,2052]{1,0:T(8,128)} %all-gather.5.cloned.1.call-done, f32[4,3072]{1,0:T(4,128)S(1)} %copy.40), kind=kOutput, calls=%fused_computation.1 | convolution fusion | flops 12902203392 | bytes 35700736 | tf_op jit(solution)/shard_map/enf,edf->nd/dot_general | solution.py:113
  321.8 0.0 copy-start.2
  321.8 0.0 reduce-scatter.2.cloned.1.call-update
  321.8 0.0 copy-start.3
  321.8 0.0 all-gather.3.cloned.1.call-start
  321.9 0.7 all-gather.3.cloned.1.call-update
  322.5 0.2 copy-done.2
  322.7 3.4 collective-permute-start
  326.2 1.2 collective-permute-done
  327.4 0.1 maximum_convert_fusion
  327.5 0.1 slice_add_fusion.1
  327.5 0.1 slice_add_fusion
  327.6 0.1 slice_add_fusion.2
  327.7 0.0 copy-done.3
  327.7 0.4 fusion.17
  328.0 16.7 %all_to_all.42 = bf16[8,128,128]{2,1,0:T(8,128)(2,1)S(1)} all-to-all(bf16[8,128,128]{2,1,0:T(8,128)(2,1)S(1)} %bitcast.74), channel_id=1, replica_groups=mesh['ep'=4,'tp'=8] {'tp'}, dimensions={0} | all-to-all | bytes 524288 | tf_op jit(solution)/shard_map/all_to_all | solution.py:89
  344.7 108.8 %reduce-scatter.2.cloned.1.call-done = bf16[384,2048]{1,0:T(8,128)(2,1)} async-done(((bf16[3072,2048]{1,0:T(8,128)(2,1)}), bf16[384,2048]{1,0:T(8,128)(2,1)}) %reduce-scatter.2.cloned.1.call-update) | async-done | bytes 1572880 | tf_op jit(solution)/shard_map/reduce_scatter | solution.py:114
  453.5 4.4 all-to-all-start.3
  457.8 0.2 copy.35
  458.0 42.9 %all-gather.3.cloned.1.call-done = bf16[1024,2048]{1,0:T(8,128)(2,1)} async-done(((bf16[128,2048]{1,0:T(8,128)(2,1)}), bf16[1024,2048]{1,0:T(8,128)(2,1)}) %all-gather.3.cloned.1.call-update) | async-done | bytes 4194320 | tf_op jit(solution)/shard_map/all_gather | solution.py:92
  500.9 0.0 copy-start.1
  500.9 3.9 convolution_convert_fusion.1
  504.8 0.0 all-to-all-done.3
  504.8 3.1 fusion.9
  507.9 0.0 copy-done.1
  (14 shorter events, 0.2 us)
Async XLA Ops:
  7.2 293.3 %copy-start = (bf16[4,2048,128]{2,1,0:T(8,128)(2,1)S(1)}, bf16[4,2048,128]{2,1,0:T(8,128)(2,1)}, u32[]{:S(2)}) copy-start(bf16[4,2048,128]{2,1,0:T(8,128)(2,1)} %param.19) | copy-start | bytes 6291460
  11.3 10.0 %all-to-all-start.2 = ((f32[4,96,4]{1,2,0:T(4,128)}), f32[4,96,4]{1,2,0:T(4,128)S(1)}, u32[]{:S(2)}, u32[]{:S(2)}) async-start(f32[4,96,4]{1,2,0:T(4,128)} %fusion.22), calls=%async_computation.2 | async-start | bytes 16384 | tf_op jit(solution)/shard_map/all_to_all | solution.py:103
  21.3 23.7 %all-to-all-start.1 = ((bf16[4,96,2048]{2,1,0:T(8,128)(2,1)}), bf16[4,96,2048]{2,1,0:T(8,128)(2,1)}, u32[]{:S(2)}, u32[]{:S(2)}) async-start(bf16[4,96,2048]{2,1,0:T(8,128)(2,1)} %bitcast.72), calls=%async_computation.1 | async-start | bytes 3145728 | tf_op jit(solution)/shard_map/all_to_all | solution.py:102
  25.7 256.4 %all-gather.5.cloned.1.call-start = ((), (), s32[]{:S(2)}) async-start(), calls=%async_computation.6 | async-start | bytes 30081024 | tf_op jit(solution)/shard_map/all_gather | solution.py:106
  48.9 404.6 %reduce-scatter.2.cloned.1.call-start = ((), (), s32[]{:S(2)}) async-start(), calls=%async_computation.7 | async-start | bytes 14155776 | tf_op jit(solution)/shard_map/reduce_scatter | solution.py:114
  321.8 0.9 copy-start.2
  321.8 5.9 %copy-start.3 = (f32[128]{0:T(128)S(1)}, f32[128]{0:T(128)}, u32[]{:S(2)}) copy-start(f32[128]{0:T(128)} %param.11) | copy-start | bytes 1540
  321.8 179.1 %all-gather.3.cloned.1.call-start = ((), (), s32[]{:S(2)}) async-start(), calls=%async_computation.5 | async-start | bytes 4718592 | tf_op jit(solution)/shard_map/all_gather | solution.py:92
  322.7 4.7 collective-permute-start
  453.5 51.3 %all-to-all-start.3 = ((bf16[4,96,2048]{2,1,0:T(8,128)(2,1)}), bf16[4,96,2048]{2,1,0:T(8,128)(2,1)}, u32[]{:S(2)}, u32[]{:S(2)}) async-start(bf16[4,96,2048]{2,1,0:T(8,128)(2,1)} %bitcast.73), calls=%async_computation.4 | async-start | bytes 3145728 | tf_op jit(solution)/shard_map/all_to_all | solution.py:115
  500.9 7.0 %copy-start.1 = (bf16[4,2048,128]{2,1,0:T(8,128)(2,1)S(1)}, bf16[4,2048,128]{2,1,0:T(8,128)(2,1)}, u32[]{:S(2)}) copy-start(bf16[4,2048,128]{2,1,0:T(8,128)(2,1)} %param.19) | copy-start | bytes 6291460
Sparse Core Ops, SparseCore 0:
  49.0 232.9 all-gather.4
  321.9 131.5 reduce-scatter.1
  455.1 45.7 all-gather.2
